TPU v7x, 512 devices: a whole 4x4x16 slice. The times are simulated.
512 devices in a mesh: fs: 16 (over z), rep: 4 (over y), tp: 8 (over x, core).
Axes of the slice: x: 4, y: 4, z: 16, core: 2. Of those that a mesh axis runs over, the one named last changes fastest.
Arguments:
- mixer_out: bfloat16 [65536, 1536], P(('fs', 'rep')), may hold values from -16 to 16
- out_grad: bfloat16 [65536, 4096], P(('fs', 'rep'), 'tp'), may hold values from -0.0234375 to 0.0234375
- factors: bfloat16 [1536, 256], P(('fs', 'rep')), may hold values from -0.15625 to 0.15625
- weight: float32 [1536, 4096], P(('fs', 'rep'), 'tp'), may hold values from -0.15625 to 0.15625
- first_moment: float32 [256, 4096], P(('fs', 'rep'), 'tp'), may hold values from -6 to 6
- second_moment: float32 [256, 4096], P(('fs', 'rep'), 'tp'), may hold values from 0.05 to 2
Outputs:
- new_weight: float32 [1536, 4096], P(('fs', 'rep'), 'tp')
- update: float32 [1536, 4096], P(('fs', 'rep'), 'tp')
- new_first: float32 [256, 4096], P(('fs', 'rep'), 'tp')
- new_second: float32 [256, 4096], P(('fs', 'rep'), 'tp')
- weight_copy: bfloat16 [1536, 4096], P(None, 'tp')
All inputs are finite; a program needn't handle non-finite values.
Results may differ from a plain program's by a relative error of at most 0.0034.
Values may be sent and summed in bfloat16 or wider, within the bound.
A program may use at most 64 MiB of HBM per device.

v0:
```python
import jax
import jax.numpy as jnp
from jax import lax
from jax.sharding import PartitionSpec as P


def in_blocks(value, dim, peers):
    before, after = (value.shape[:dim], value.shape[dim + 1 :])
    return jnp.moveaxis(value.reshape(*before, peers, -1, *after), dim, 0)


def sent_and_summed(value, axis, dim):
    peers = lax.axis_size(axis)
    pieces = lax.all_to_all(in_blocks(value, dim, peers), axis, 0, 0, tiled=True)
    return jnp.sum(pieces, axis=0)


def in_one_piece(arrays, axis, dim, along):
    ends, at = ([], 0)
    for a in arrays[:-1]:
        at += a.shape[along]
        ends.append(at)
    both = jnp.concatenate(arrays, axis=along)
    return tuple(jnp.split(lax.all_gather(both, axis, axis=dim, tiled=True), ends, axis=along))


def sent_to_all(value, axis):
    copies = jnp.broadcast_to(value, (lax.axis_size(axis), *value.shape))
    return lax.all_to_all(copies, axis, split_axis=0, concat_axis=0, tiled=True)


def taken_together(value, axis):
    everything = sent_to_all(value, axis)
    return jnp.sum(everything, axis=0)


def packed_total(arrays, axis):
    ravelled, at, outs = (jnp.concatenate([a.reshape(-1) for a in arrays]), 0, [])
    total = taken_together(ravelled, axis)
    for a in arrays:
        outs.append(total[at : at + a.size].reshape(a.shape))
        at += a.size
    return tuple(outs)


def whole_of(value, axes, dim):
    for axis in reversed(axes):
        value = lax.all_gather(value, axis, axis=dim, tiled=True)
    return value


def contract_rows(left, right):
    return lax.dot_general(
        left, right, (((0,), (0,)), ((), ())), preferred_element_type=jnp.float32
    )


def per_device(mixer_out, out_grad, factors, weight, first_moment, second_moment):
    columns = mixer_out
    partial_value = lax.psum_scatter(
        contract_rows(columns, out_grad), "fs", scatter_dimension=0, tiled=True
    )
    gradient = sent_and_summed(partial_value, "rep", 0)
    grad_low = gradient.astype(jnp.bfloat16)
    columns = factors
    projected = sent_and_summed(contract_rows(columns, grad_low), ("fs", "rep"), 0)
    new_first = 0.8 * first_moment + 0.2 * projected
    new_second = 0.9 * second_moment + 0.1 * projected * projected
    direction = new_first / (jnp.sqrt(new_second) + 1e-08)
    dir_low = direction.astype(jnp.bfloat16)
    proj_low = projected.astype(jnp.bfloat16)
    dir_whole, proj_whole = in_one_piece((dir_low, proj_low), ("fs", "rep"), 0, 1)
    dir_wide = dir_whole.astype(jnp.float32)
    proj_wide = proj_whole.astype(jnp.float32)
    dir_sum, proj_sum = packed_total(
        (jnp.sum(dir_wide * dir_wide), jnp.sum(proj_wide * proj_wide)), "tp"
    )
    back_dir = jnp.dot(factors, dir_whole, preferred_element_type=jnp.float32)
    back_proj = jnp.dot(factors, proj_whole, preferred_element_type=jnp.float32)
    scale_ratio = jnp.sqrt(dir_sum) / jnp.sqrt(proj_sum + 1e-06)
    update = back_dir + scale_ratio * (gradient - back_proj)
    new_weight = weight - 0.01 * update
    weight_copy = whole_of(new_weight.astype(jnp.bfloat16), ("fs", "rep"), 0)
    return (new_weight, update, new_first, new_second, weight_copy)


def solution(mesh):
    in_specs = (
        P(("fs", "rep"), None),
        P(("fs", "rep"), "tp"),
        P(("fs", "rep"), None),
        P(("fs", "rep"), "tp"),
        P(("fs", "rep"), "tp"),
        P(("fs", "rep"), "tp"),
    )
    out_specs = (
        P(("fs", "rep"), "tp"),
        P(("fs", "rep"), "tp"),
        P(("fs", "rep"), "tp"),
        P(("fs", "rep"), "tp"),
        P(None, "tp"),
    )
    return jax.shard_map(
        per_device, mesh=mesh, in_specs=in_specs, out_specs=out_specs, check_vma=False
    )
```

profile of v0, /device:TPU:24, one launch (start us, length us, event | category | flops | bytes accessed | tf_op | source)
XLA Modules:
  0.0 355.8 jit_solution(12526476906708309702)
XLA Ops:
  7.2 0.0 copy-start
  7.2 0.0 reduce-scatter.2.cloned.1.call-start
  7.2 1.8 copy-done
  9.1 4.7 %fusion.11 = f32[1536,512]{1,0:T(8,128)} fusion(bf16[1024,1536]{1,0:T(8,128)(2,1)S(1)} %copy-done, bf16[1024,512]{1,0:T(8,128)(2,1)} %param.7), kind=kOutput, calls=%fused_computation.21 | convolution fusion | flops 1610612736 | bytes 7340032 | tf_op jit(solution)/shard_map/dot_general | solution.py:53
  13.8 0.0 copy-start.1
  13.8 0.0 copy-start.3
  13.8 0.0 copy-start.4
  13.8 0.0 reduce-scatter.2.cloned.1.call-update
  13.8 0.0 all-gather.3.cloned.1.call-start
  13.9 81.3 %reduce-scatter.2.cloned.1.call-done = f32[96,512]{1,0:T(8,128)} async-done(((f32[1536,512]{1,0:T(8,128)}), f32[96,512]{1,0:T(8,128)}) %reduce-scatter.2.cloned.1.call-update) | async-done | bytes 196624 | tf_op jit(solution)/shard_map/reduce_scatter | solution.py:60
  95.1 0.0 copy-start.2
  95.1 9.0 %all_to_all.16 = f32[4,24,512]{2,1,0:T(8,128)S(1)} all-to-all(f32[4,24,512]{2,1,0:T(8,128)} %bitcast.23), channel_id=1, replica_groups=mesh['fs'=16,'rep'=4,'tp'=8] {'rep'}, dimensions={0} | all-to-all | bytes 393216 | tf_op jit(solution)/shard_map/all_to_all | solution.py:14
  104.2 0.0 copy-done.1
  104.2 1.1 convolution_bitcast_fusion
  105.3 2.0 reshape.34
  107.2 35.2 %all_to_all.17 = f32[64,4,512]{2,1,0:T(4,128)} all-to-all(f32[64,4,512]{2,1,0:T(4,128)} %reshape.34), channel_id=1, replica_groups=mesh['fs'=16,'rep'=4,'tp'=8] {'fs','rep'}, dimensions={0} | all-to-all | bytes 1048576 | tf_op jit(solution)/shard_map/all_to_all | solution.py:14
  142.4 1.2 reduce_sum.46
  143.6 0.0 copy-done.3
  143.6 0.0 copy-done.4
  143.6 0.6 fusion.7
  144.2 106.1 %all-gather = bf16[64,4,1024]{2,1,0:T(4,128)(2,1)} all-gather(bf16[1,4,1024]{2,1,0:T(4,128)(2,1)S(1)} %maximum_bitcast_fusion), channel_id=1, replica_groups=mesh['fs'=16,'rep'=4,'tp'=8] {'fs','rep'}, dimensions={0}, use_global_device_ids=true | all-gather | bytes 532480 | tf_op jit(solution)/shard_map/all_gather | solution.py:24
  250.4 2.0 reshape.38
  252.3 1.8 multiply_reduce_fusion.1
  254.1 1.4 pad_maximum_fusion
  255.5 9.4 %all_to_all.18 = f32[8,1,2]{2,1,0:T(1,128)S(1)} all-to-all(f32[8,1,2]{2,1,0:T(1,128)S(1)} %broadcast_in_dim.3), channel_id=1, replica_groups=mesh['fs'=16,'rep'=4,'tp'=8] {'tp'}, dimensions={0} | all-to-all | bytes 128 | tf_op jit(solution)/shard_map/all_to_all | solution.py:29
  264.9 0.6 fusion.10
  266.8 1.1 fusion.2
  267.9 0.0 copy-done.2
  267.9 1.7 fusion.8
  269.7 12.7 %all_gather.10 = bf16[96,512]{1,0:T(8,128)(2,1)} all-gather(bf16[24,512]{1,0:T(8,128)(2,1)S(1)} %get-tuple-element.7), channel_id=1, replica_groups=mesh['fs'=16,'rep'=4,'tp'=8] {'rep'}, dimensions={0}, use_global_device_ids=true | all-gather | bytes 122880 | tf_op jit(solution)/shard_map/all_gather | solution.py:48
  282.3 0.0 all-gather.3.cloned.1.call-update
  282.4 63.9 %all-gather.3.cloned.1.call-done = bf16[1536,512]{1,0:T(8,128)(2,1)} async-done(((bf16[96,512]{1,0:T(8,128)(2,1)}), bf16[1536,512]{1,0:T(8,128)(2,1)}) %all-gather.3.cloned.1.call-update) | async-done | bytes 1572880 | tf_op jit(solution)/shard_map/all_gather | solution.py:48
  346.3 2.7 copy.16
  (4 shorter events, 0.1 us)
Async XLA Ops:
  7.2 1.9 copy-start
  7.2 87.9 %reduce-scatter.2.cloned.1.call-start = ((), (), s32[]{:S(2)}) async-start(), calls=%async_computation.4 | async-start | bytes 3342336 | tf_op jit(solution)/shard_map/reduce_scatter | solution.py:60
  13.8 90.4 %copy-start.1 = (bf16[24,256]{1,0:T(8,128)(2,1)S(1)}, bf16[24,256]{1,0:T(8,128)(2,1)}, u32[]{:S(2)}) copy-start(bf16[24,256]{1,0:T(8,128)(2,1)} %param.8) | copy-start | bytes 36868
  13.8 129.8 %copy-start.3 = (f32[4,512]{1,0:T(4,128)S(1)}, f32[4,512]{1,0:T(4,128)}, u32[]{:S(2)}) copy-start(f32[4,512]{1,0:T(4,128)} %param.11) | copy-start | bytes 24580
  13.8 129.8 %copy-start.4 = (f32[4,512]{1,0:T(4,128)S(1)}, f32[4,512]{1,0:T(4,128)}, u32[]{:S(2)}) copy-start(f32[4,512]{1,0:T(4,128)} %param.10) | copy-start | bytes 24580
  13.8 332.5 %all-gather.3.cloned.1.call-start = ((), (), s32[]{:S(2)}) async-start(), calls=%async_computation.5 | async-start | bytes 1671168 | tf_op jit(solution)/shard_map/all_gather | solution.py:48
  95.1 172.8 %copy-start.2 = (f32[24,512]{1,0:T(8,128)S(1)}, f32[24,512]{1,0:T(8,128)}, u32[]{:S(2)}) copy-start(f32[24,512]{1,0:T(8,128)} %param.9) | copy-start | bytes 147460
Sparse Core Ops, SparseCore 0:
  13.9 81.1 reduce-scatter.1
  282.5 63.7 all-gather.2
where the time goes:
time: 357 us; the launch traced here: 356 us
  blocking collectives  172 us (48%)
  waiting for transfers between devices  145 us (41%)
  between operations  15.5 us (4%)
  local copies, waits for them, and re-layouts  9.04 us (3%)
  matrix products  8.62 us (2%)
  other arithmetic  4.95 us (1%)
    all_gather x1, blocking collectives, in_one_piece(): lax.all_gather(both, axis, axis=dim, tiled=True)  106 us
    reduce_scatter x1, waiting for transfers between devices, per_device(): lax.psum_scatter(contract_rows(columns, out_grad), 'fs', scatter_dimensio...  81.3 us
    all_gather x1, waiting for transfers between devices, whole_of(): value = lax.all_gather(value, axis, axis=dim, tiled=True)  63.9 us
    all_to_all x2, blocking collectives, sent_and_summed(): lax.all_to_all(in_blocks(value, dim, peers), axis, 0, 0, tiled=True)  44.3 us
    all_gather x1, blocking collectives, whole_of(): value = lax.all_gather(value, axis, axis=dim, tiled=True)  12.7 us
    all_to_all x1, blocking collectives, sent_to_all(): return lax.all_to_all(copies, axis, split_axis=0, concat_axis=0, tiled=True)  9.36 us
  transfers between devices with their start and end apart: 2, of which 2 were waited for; matrix products, arithmetic and copies ran while one was open for 0% of the time, Pallas kernels for 0%

commit v1 on v0

v1 whole, which is shorter than its diff:
```python
import jax
import jax.numpy as jnp
from jax import lax
from jax.experimental import pallas as pl
from jax.experimental.pallas import tpu as pltpu
from jax.sharding import PartitionSpec as P

MESH = pl.DeviceIdType.MESH
F32, BF16 = jnp.float32, jnp.bfloat16
WINDOW = ((1, 15, 2), (1, 15, 14))
YS = (1, 3, 2)
N_SEM = 160


def pack(v):
    low = jnp.concatenate([v[16:24, 0:128], v[16:24, 128:256]], axis=0)
    return jnp.concatenate([v[0:16], low], axis=1)


def unpack(v):
    low = jnp.concatenate([v[0:8, 256:384], v[8:16, 256:384]], axis=1)
    return jnp.concatenate([v[0:16, 0:256], low], axis=0)


def rows_dot(a, b):
    return lax.dot_general(a, b, (((0,), (0,)), ((), ())), preferred_element_type=F32)


def kernel(mixer, og, fac, w, m1, m2, nw_o, up_o, nf_o, ns_o, wc_o,
           gf, sy, ry, gy, sa, ra, ga, sb, rb, fall, f32s, pp, spy, rpy, spa, rpa, pb, m1a, m2a, dall, pick, mom, sums,
           wall, ssem, rsem):
    z, y, t = lax.axis_index("fs"), lax.axis_index("rep"), lax.axis_index("tp")
    q, r = z // 4, lax.rem(z, 4)

    def zd(d):
        return {"fs": lax.rem(z + d, 16)}

    def yd(d):
        return {"rep": lax.rem(y + d, 4)}

    def td(d):
        return {"tp": lax.rem(t + d, 8)}

    copies = []

    def send(src, dst, dev):
        i = len(copies)
        c = pltpu.make_async_remote_copy(src_ref=src, dst_ref=dst, send_sem=ssem.at[i], recv_sem=rsem.at[i],
                                         device_id=dev, device_id_type=MESH)
        c.start()
        copies.append(c)
        return c

    def rows(index, size):
        return pl.ds(pl.multiple_of(index * size, size), size)

    barrier = pltpu.get_barrier_semaphore()
    peers = [zd(d) for d in (1, 15, 2, 14, 4, 8, 12)] + [yd(d) for d in YS] + [td(d) for d in range(1, 8)]
    for dev in peers:
        pl.semaphore_signal(barrier, inc=1, device_id=dev, device_id_type=MESH)
    pl.semaphore_wait(barrier, len(peers))

    m1a[q] = m1[...]
    m2a[q] = m2[...]
    src = lax.broadcasted_iota(jnp.int32, (256, 256), 0)
    dst = lax.broadcasted_iota(jnp.int32, (256, 256), 1)
    ky = dst // 64
    rest = dst - ky * 64
    kr = rest // 16
    rest = rest - kr * 16
    kk = rest // 4
    order = kk * 64 + kr * 16 + ky * 4 + (rest - kk * 4)
    swap = jnp.where(src == order, 1.0, 0.0).astype(BF16)
    fac_p = jnp.dot(fac[...], swap, preferred_element_type=F32)
    fall[r, q] = pack(fac_p).astype(BF16)
    fb, mb = [], []
    for j in (1, 3, 2):
        fb.append(send(fall.at[r, q], fall.at[r, q], zd(4 * j)))
    for j in (1, 3, 2):
        mb.append(send(m1a.at[q], m1a.at[q], zd(4 * j)))
        mb.append(send(m2a.at[q], m2a.at[q], zd(4 * j)))

    for k in range(4):
        tile = rows_dot(mixer[:, 384 * k:384 * k + 384], og[...])
        for rr in range(4):
            for yy in range(4):
                at = 96 * rr + 24 * yy
                to = yy * 384 + rr * 96 + k * 24
                for c in range(2):
                    gf[c, to:to + 24, :] = tile[at:at + 24, 256 * c:256 * c + 256]
    gy_copies = []
    for c in range(2):
        sy[c] = gf[c].astype(BF16)
        gy_copies.append([send(sy.at[c, rows(lax.rem(y + d, 4), 384)], ry.at[c, j], yd(d)) for j, d in enumerate(YS)])

    for c in fb:
        c.wait_recv()
    fa = [send(fall.at[r], fall.at[r], zd(1)), send(fall.at[r], fall.at[r], zd(15)),
          send(fall.at[r, pl.ds(0, 2)], fall.at[r, pl.ds(0, 2)], zd(2)),
          send(fall.at[r, pl.ds(2, 2)], fall.at[r, pl.ds(2, 2)], zd(14))]
    for c in fa:
        c.wait_recv()
    for rr in range(4):
        for k in range(4):
            f32s[rr * 96 + k * 24:rr * 96 + k * 24 + 24, :] = unpack(fall[rr, k].astype(F32))
    fy = f32s[...].astype(BF16)

    ga_copies, py_copies = [], []
    for c in range(2):
        for x in gy_copies[c]:
            x.wait_recv()
        total = gf[c, rows(y, 384), :]
        for j in range(3):
            total = total + ry[c, j].astype(F32)
        gy[c] = total
        low = total.astype(BF16)
        sa[c] = low
        part = rows_dot(fy, low)
        pp[c] = part
        spy[c] = part.astype(BF16)
        py_copies.append([send(spy.at[c, rows(lax.rem(y + d, 4), 64)], rpy.at[c, j], yd(d)) for j, d in enumerate(YS)])
        ga_copies.append([send(sa.at[c, rows(lax.rem(z + d, 4), 96)], ra.at[c, j], zd(d))
                          for j, d in enumerate(WINDOW[c])])

    pa_copies, pb_copies, gb_copies = [], [], []
    for c in range(2):
        for x in py_copies[c]:
            x.wait_recv()
        total = pp[c, rows(y, 64), :]
        for j in range(3):
            total = total + rpy[c, j].astype(F32)
        spa[c] = total
        pa_copies.append([send(spa.at[c, rows(lax.rem(z + d, 4), 16)], rpa.at[c, j], zd(d))
                          for j, d in enumerate(WINDOW[c])])
    for c in range(2):
        for x in pa_copies[c]:
            x.wait_recv()
        total = spa[c, rows(r, 16), :]
        for j in range(3):
            total = total + rpa[c, j]
        pb[c, q] = total
        pb_copies.append([send(pb.at[c, q], pb.at[c, q], zd(4 * j)) for j in (1, 3, 2)])
        for x in ga_copies[c]:
            x.wait_recv()
        total = gy[c, rows(r, 96), :]
        for j in range(3):
            total = total + ra[c, j].astype(F32)
        ga[c] = total
        for k in range(4):
            sb[c, k] = pack(total[24 * k:24 * k + 24]).astype(BF16)
        gb_copies.append([send(sb.at[c, lax.rem(q + j, 4)], rb.at[c, j - 1], zd(4 * j)) for j in (1, 3, 2)])

    for x in mb:
        x.wait_recv()
    proj = []
    for c in range(2):
        for x in pb_copies[c]:
            x.wait_recv()
        proj.append(((pb[c, 0] + pb[c, 1]) + pb[c, 2]) + pb[c, 3])
    proj = jnp.concatenate(proj, axis=1)
    for k in range(4):
        pick[0, 4 * k:4 * k + 4, :] = m1a[k]
        pick[1, 4 * k:4 * k + 4, :] = m2a[k]
    first = 0.8 * pick[0] + 0.2 * proj
    second = 0.9 * pick[1] + 0.1 * proj * proj
    direction = first / (jnp.sqrt(second) + 1e-08)
    dall[0, y, r] = direction.astype(BF16)
    dall[1, y, r] = proj.astype(BF16)
    da = []
    for d in (1, 15):
        for p in range(2):
            da.append(send(dall.at[p, y, r], dall.at[p, y, r], zd(d)))
    for d, at in ((2, 0), (14, 256)):
        for p in range(2):
            here = dall.at[p, y, r, :, pl.ds(at, 256)]
            da.append(send(here, here, zd(d)))
    for k in range(4):
        mom[0, k] = first[4 * k:4 * k + 4]
        mom[1, k] = second[4 * k:4 * k + 4]
    nf_o[...] = mom[0, q]
    ns_o[...] = mom[1, q]
    for x in da:
        x.wait_recv()
    dy = [send(dall.at[p, y], dall.at[p, y], yd(d)) for d in YS for p in range(2)]

    grad = []
    for c in range(2):
        for x in gb_copies[c]:
            x.wait_recv()
        total = ga[c, rows(q, 24), :]
        for j in range(3):
            total = total + unpack(rb[c, j].astype(F32))
        grad.append(total)
    grad = jnp.concatenate(grad, axis=1)

    for x in dy:
        x.wait_recv()
    both = []
    for p in range(2):
        both.append(dall[p].reshape(256, 512))
        wide = both[p].astype(F32)
        sq = (wide * wide).reshape(32, 8, 512).sum(axis=0)
        sums[t, p] = sq[:, 0:128] + sq[:, 128:256] + sq[:, 256:384] + sq[:, 384:512]
    st = [send(sums.at[t], sums.at[t], td(d)) for d in range(1, 8)]
    mine = fac_p.astype(BF16)
    back_dir = jnp.dot(mine, both[0], preferred_element_type=F32)
    back_proj = jnp.dot(mine, both[1], preferred_element_type=F32)
    for x in st:
        x.wait_recv()
    totals = []
    for p in range(2):
        s = sums[0, p]
        for i in range(1, 8):
            s = s + sums[i, p]
        totals.append(jnp.sum(jnp.sum(s, axis=1, keepdims=True), axis=0, keepdims=True))
    scale = jnp.sqrt(totals[0]) / jnp.sqrt(totals[1] + 1e-06)
    update = back_dir + scale * (grad - back_proj)
    up_o[...] = update
    new_w = w[...] - 0.01 * update
    nw_o[...] = new_w
    wall[y, r, q] = jnp.concatenate([pack(new_w[:, 0:256]), pack(new_w[:, 256:512])], axis=1).astype(BF16)

    def block(dz, j):
        zz = lax.rem(z + 16 - dz, 16)
        return lax.rem(zz, 4), lax.rem(zz // 4 + 4 - j, 4)

    last = []

    def spread(rr, kk):
        for d in YS:
            last.append(send(wall.at[y, rr, kk], wall.at[y, rr, kk], yd(d)))

    first_b = {j: send(wall.at[y, r, q], wall.at[y, r, q], zd(4 * j)) for j in (2, 1, 3)}
    second_a = {}

    def around(j):
        rr, kk = block(0, j)
        to = {0: (1, 15, 2, 14), 1: (1, 15, 2), 3: (1, 15, 14), 2: (1, 15)}[j]
        for d in to:
            second_a[j, d] = send(wall.at[y, rr, kk], wall.at[y, rr, kk], zd(d))
        return to

    def landed(j, to):
        for d in to:
            second_a[j, d].wait_recv()
            spread(*block(d, j))

    to = around(0)
    spread(r, q)
    landed(0, to)
    for j in (1, 3):
        first_b[j].wait_recv()
        to = around(j)
        spread(*block(0, j))
        landed(j, to)
    first_b[2].wait_recv()
    to = around(2)
    spread(*block(0, 2))
    landed(2, to)
    for x in last:
        x.wait_recv()
    for k in range(4):
        for rr in range(4):
            at = 96 * (4 * k + rr)
            out = []
            for yy in range(4):
                v = wall[yy, rr, k].astype(F32)
                out.append(jnp.concatenate([unpack(v[:, 0:384]), unpack(v[:, 384:768])], axis=1))
            wc_o[at:at + 96, :] = jnp.concatenate(out, axis=0).astype(BF16)
    for x in copies:
        x.wait_send()


def per_device(*args):
    v = pl.BlockSpec(memory_space=pltpu.VMEM)
    shape = jax.ShapeDtypeStruct
    return pl.pallas_call(
        kernel,
        name="step",
        out_shape=(shape((24, 512), F32), shape((24, 512), F32), shape((4, 512), F32), shape((4, 512), F32),
                   shape((1536, 512), BF16)),
        in_specs=[v] * 6,
        out_specs=[v] * 5,
        scratch_shapes=[
            pltpu.VMEM((2, 1536, 256), F32),
            pltpu.VMEM((2, 1536, 256), BF16),
            pltpu.VMEM((2, 3, 384, 256), BF16),
            pltpu.VMEM((2, 384, 256), F32),
            pltpu.VMEM((2, 384, 256), BF16),
            pltpu.VMEM((2, 3, 96, 256), BF16),
            pltpu.VMEM((2, 96, 256), F32),
            pltpu.VMEM((2, 4, 16, 384), BF16),
            pltpu.VMEM((2, 3, 16, 384), BF16),
            pltpu.VMEM((4, 4, 16, 384), BF16),
            pltpu.VMEM((384, 256), F32),
            pltpu.VMEM((2, 256, 256), F32),
            pltpu.VMEM((2, 256, 256), BF16),
            pltpu.VMEM((2, 3, 64, 256), BF16),
            pltpu.VMEM((2, 64, 256), F32),
            pltpu.VMEM((2, 3, 16, 256), F32),
            pltpu.VMEM((2, 4, 16, 256), F32),
            pltpu.VMEM((4, 4, 512), F32),
            pltpu.VMEM((4, 4, 512), F32),
            pltpu.VMEM((2, 4, 4, 16, 512), BF16),
            pltpu.VMEM((2, 16, 512), F32),
            pltpu.VMEM((2, 4, 4, 512), F32),
            pltpu.VMEM((8, 2, 8, 128), F32),
            pltpu.VMEM((4, 4, 4, 16, 768), BF16),
            pltpu.SemaphoreType.DMA((N_SEM,)),
            pltpu.SemaphoreType.DMA((N_SEM,)),
        ],
        compiler_params=pltpu.CompilerParams(collective_id=0, has_side_effects=True, vmem_limit_bytes=56 * 1024 * 1024),
    )(*args)


def solution(mesh):
    both = ("fs", "rep")
    in_specs = (P(both, None), P(both, "tp"), P(both, None), P(both, "tp"), P(both, "tp"), P(both, "tp"))
    out_specs = (P(both, "tp"), P(both, "tp"), P(both, "tp"), P(both, "tp"), P(None, "tp"))
    return jax.shard_map(per_device, mesh=mesh, in_specs=in_specs, out_specs=out_specs, check_vma=False)
```

time: 357 us -> 113 us (0.32)
  blocking collectives: 172 us -> 0 us
  waiting for transfers between devices: 145 us -> 0 us
  Pallas kernels: 0 us -> 103 us
  between operations: 15.5 us -> 0.64 us
  matrix products: 8.62 us -> 0 us
  other arithmetic: 4.95 us -> 0 us
    all_gather x2 -> x0, blocking collectives: 119 us -> none  [the longest x1 106 us: in_one_piece(): lax.all_gather(both, axis, axis=dim, tiled=True)]
    pallas_call x0 -> x1, Pallas kernels: none -> 103 us  [per_device(): pl.pallas_call(kernel, name='step', out_shape=(shape((24, 512), F32), sha...]
    reduce_scatter x1 -> x0, waiting for transfers between devices: 81.3 us -> none  [per_device(): lax.psum_scatter(contract_rows(columns, out_grad), 'fs', scatter_dimensio...]
    all_gather x1 -> x0, waiting for transfers between devices: 63.9 us -> none  [whole_of(): value = lax.all_gather(value, axis, axis=dim, tiled=True)]
    all_to_all x3 -> x0, blocking collectives: 53.6 us -> none  [the longest x2 44.3 us: sent_and_summed(): lax.all_to_all(in_blocks(value, dim, peers), axis, 0, 0, tiled=True)]
    dot_general x4 -> x0, matrix products: 8.62 us -> none  [the longest x2 5.78 us: contract_rows(): lax.dot_general(left, right, (((0,), (0,)), ((), ())), preferred_element_...]
    unnamed x12 -> x5, local copies, waits for them, and re-layouts: 6.47 us -> 8.08 us
  transfers between devices with their start and end apart: 2 -> 0, of which waited for: 2 -> 0; matrix products, arithmetic and copies ran while one was open for 0% -> 0% of each run, Pallas kernels for 0% -> 0%
where the time goes in v1:
time: 113 us; the launch traced here: 111 us
  Pallas kernels  103 us (91%)
  local copies, waits for them, and re-layouts  8.08 us (7%)
    pallas_call x1, Pallas kernels, per_device(): pl.pallas_call(kernel, name='step', out_shape=(shape((24, 512), F32), sha...  103 us
    unnamed x5, local copies, waits for them, and re-layouts  8.08 us

profile of v1, /device:TPU:24, one launch (start us, length us, event | category | flops | bytes accessed | tf_op | source)
XLA Modules:
  0.0 111.3 jit_solution(16955028866126828122)
XLA Ops:
  0.6 102.6 %step.1 = (f32[24,512]{1,0:T(8,128)}, f32[24,512]{1,0:T(8,128)}, f32[4,512]{1,0:T(4,128)}, f32[4,512]{1,0:T(4,128)}, bf16[1536,512]{1,0:T(8,128)(2,1)}) custom-call(bf16[1024,1536]{1,0:T(8,128)(2,1)} %mixer.1, bf16[1024,512]{1,0:T(8,128)(2,1)} %og.1, bf16[24,256]{1,0:T(8,128)(2,1)} %fac.1, f32[24,512]{1,0:T(8,128)} %w.1, f32[4,512]{1,0:T(4,128)} %m1.1, ...), custom_call_target="tpu_custom_call" | custom-call | tf_op jit(solution)/shard_map/step/pallas_call | solution.py:277
  103.2 1.4 %copy.16 = f32[24,512]{1,0:T(8,128)} copy(f32[24,512]{1,0:T(8,128)} %get-tuple-element.10) | data formatting | bytes 98304
  104.6 1.4 %copy.17 = f32[24,512]{1,0:T(8,128)} copy(f32[24,512]{1,0:T(8,128)} %get-tuple-element.11) | data formatting | bytes 98304
  106.1 1.3 %copy.18 = f32[4,512]{1,0:T(4,128)} copy(f32[4,512]{1,0:T(4,128)} %get-tuple-element.12) | data formatting | bytes 16384
  107.4 1.3 %copy.19 = f32[4,512]{1,0:T(4,128)} copy(f32[4,512]{1,0:T(4,128)} %get-tuple-element.13) | data formatting | bytes 16384
  108.7 2.7 %copy.20 = bf16[1536,512]{1,0:T(8,128)(2,1)} copy(bf16[1536,512]{1,0:T(8,128)(2,1)} %get-tuple-element.14) | data formatting | bytes 3145728

commit v2 on v1

--- a/solution.py
+++ b/solution.py
@@ -9,7 +9,7 @@
 F32, BF16 = jnp.float32, jnp.bfloat16
 WINDOW = ((1, 15, 2), (1, 15, 14))
 YS = (1, 3, 2)
-N_SEM = 160
+N_SEM = 192
 
 
 def pack(v):
@@ -26,9 +26,9 @@
     return lax.dot_general(a, b, (((0,), (0,)), ((), ())), preferred_element_type=F32)
 
 
-def kernel(mixer, og, fac, w, m1, m2, nw_o, up_o, nf_o, ns_o, wc_o,
-           gf, sy, ry, gy, sa, ra, ga, sb, rb, fall, f32s, pp, spy, rpy, spa, rpa, pb, m1a, m2a, dall, pick, mom, sums,
-           wall, ssem, rsem):
+def kernel(mixer_h, og_h, fac_h, w_h, m1_h, m2_h, out_o, wc_o,
+           mixer, og, fac, w, mom, turned, gf, sy, relay, direct, joined, landed_j, gy, sa, ra, ga, sb, rb, fall, f32s,
+           pp, spy, rpy, spa, rpa, pb, m1a, m2a, dall, pick, sums, klass, ysum, wall, isem, ssem, rsem):
     z, y, t = lax.axis_index("fs"), lax.axis_index("rep"), lax.axis_index("tp")
     q, r = z // 4, lax.rem(z, 4)
 
@@ -58,10 +58,38 @@
     peers = [zd(d) for d in (1, 15, 2, 14, 4, 8, 12)] + [yd(d) for d in YS] + [td(d) for d in range(1, 8)]
     for dev in peers:
         pl.semaphore_signal(barrier, inc=1, device_id=dev, device_id_type=MESH)
-    pl.semaphore_wait(barrier, len(peers))
-
-    m1a[q] = m1[...]
-    m2a[q] = m2[...]
+
+    def load(i, src, dst):
+        c = pltpu.make_async_copy(src, dst, isem.at[i])
+        c.start()
+        return c
+
+    tiles = [pl.ds(384 * k, 384) for k in range(4)]
+    in_og = load(0, og_h, og)
+    in_mixer = [load(1 + k, mixer_h.at[:, tiles[k]], mixer.at[:, tiles[k]]) for k in range(4)]
+    in_fac = load(5, fac_h, fac)
+    in_m1 = load(6, m1_h, m1a.at[q])
+    in_m2 = load(7, m2_h, m2a.at[q])
+    in_w = load(8, w_h, w)
+
+    def partial(c):
+        cols = pl.ds(256 * c, 256)
+        for k in range(4):
+            if c == 0:
+                in_mixer[k].wait()
+                turned[k] = mixer[:, tiles[k]].T
+            tile = jnp.dot(turned[k], og[:, cols], preferred_element_type=F32)
+            for rr in range(4):
+                for yy in range(4):
+                    at = 96 * rr + 24 * yy
+                    to = yy * 384 + rr * 96 + k * 24
+                    gf[c, to:to + 24, :] = tile[at:at + 24]
+        sy[c] = gf[c].astype(BF16)
+
+    in_og.wait()
+    partial(0)
+    in_fac.wait()
+
     src = lax.broadcasted_iota(jnp.int32, (256, 256), 0)
     dst = lax.broadcasted_iota(jnp.int32, (256, 256), 1)
     ky = dst // 64
@@ -73,25 +101,37 @@
     swap = jnp.where(src == order, 1.0, 0.0).astype(BF16)
     fac_p = jnp.dot(fac[...], swap, preferred_element_type=F32)
     fall[r, q] = pack(fac_p).astype(BF16)
+    in_m1.wait()
+    in_m2.wait()
+    pl.semaphore_wait(barrier, len(peers))
+
+    def piece(d, half):
+        return pl.ds(pl.multiple_of(lax.rem(y + d, 4) * 384 + 192 * half, 192), 192)
+
+    def step_one(c):
+        up = [send(sy.at[c, piece(2, 0)], relay.at[c, 0], yd(1)), send(sy.at[c, piece(1, 1)], direct.at[c, 0], yd(1))]
+        down = [send(sy.at[c, piece(2, 1)], relay.at[c, 1], yd(3)), send(sy.at[c, piece(3, 0)], direct.at[c, 1], yd(3))]
+        return up[0], down[0], up[1], down[1]
+
+    def step_two(c, first):
+        out = []
+        for i, d in ((0, 1), (1, 3)):
+            first[i].wait_recv()
+            joined[c, i] = (gf[c, piece(d, i), :] + relay[c, i].astype(F32)).astype(BF16)
+            out.append(send(joined.at[c, i], landed_j.at[c, i], yd(d)))
+        return list(first[2:]) + out
+
+    ones, twos = [None, None], [None, None]
+    ones[0] = step_one(0)
     fb, mb = [], []
     for j in (1, 3, 2):
         fb.append(send(fall.at[r, q], fall.at[r, q], zd(4 * j)))
     for j in (1, 3, 2):
         mb.append(send(m1a.at[q], m1a.at[q], zd(4 * j)))
         mb.append(send(m2a.at[q], m2a.at[q], zd(4 * j)))
-
-    for k in range(4):
-        tile = rows_dot(mixer[:, 384 * k:384 * k + 384], og[...])
-        for rr in range(4):
-            for yy in range(4):
-                at = 96 * rr + 24 * yy
-                to = yy * 384 + rr * 96 + k * 24
-                for c in range(2):
-                    gf[c, to:to + 24, :] = tile[at:at + 24, 256 * c:256 * c + 256]
-    gy_copies = []
-    for c in range(2):
-        sy[c] = gf[c].astype(BF16)
-        gy_copies.append([send(sy.at[c, rows(lax.rem(y + d, 4), 384)], ry.at[c, j], yd(d)) for j, d in enumerate(YS)])
+    partial(1)
+    twos[0] = step_two(0, ones[0])
+    ones[1] = step_one(1)
 
     for c in fb:
         c.wait_recv()
@@ -107,11 +147,13 @@
 
     ga_copies, py_copies = [], []
     for c in range(2):
-        for x in gy_copies[c]:
-            x.wait_recv()
-        total = gf[c, rows(y, 384), :]
-        for j in range(3):
-            total = total + ry[c, j].astype(F32)
+        if c == 1:
+            twos[1] = step_two(1, ones[1])
+        for x in twos[c]:
+            x.wait_recv()
+        total = jnp.concatenate(
+            [gf[c, piece(0, 0), :] + landed_j[c, 0].astype(F32) + direct[c, 1].astype(F32),
+             gf[c, piece(0, 1), :] + landed_j[c, 1].astype(F32) + direct[c, 0].astype(F32)], axis=0)
         gy[c] = total
         low = total.astype(BF16)
         sa[c] = low
@@ -166,22 +208,50 @@
     direction = first / (jnp.sqrt(second) + 1e-08)
     dall[0, y, r] = direction.astype(BF16)
     dall[1, y, r] = proj.astype(BF16)
-    da = []
+    da = {}
     for d in (1, 15):
-        for p in range(2):
-            da.append(send(dall.at[p, y, r], dall.at[p, y, r], zd(d)))
+        da[d] = [send(dall.at[p, y, r], dall.at[p, y, r], zd(d)) for p in range(2)]
     for d, at in ((2, 0), (14, 256)):
-        for p in range(2):
-            here = dall.at[p, y, r, :, pl.ds(at, 256)]
-            da.append(send(here, here, zd(d)))
+        here = [dall.at[p, y, r, :, pl.ds(at, 256)] for p in range(2)]
+        da[d] = [send(here[p], here[p], zd(d)) for p in range(2)]
+    dy = []
+
+    def on(rr):
+        for d in YS:
+            for p in range(2):
+                dy.append(send(dall.at[p, y, rr], dall.at[p, y, rr], yd(d)))
+
+    for p in range(2):
+        wide = dall[p, y, r].astype(F32)
+        sq = wide * wide
+        sq = sq[0:8] + sq[8:16]
+        sums[t, p] = sq[:, 0:128] + sq[:, 128:256] + sq[:, 256:384] + sq[:, 384:512]
+    st = [send(sums.at[t], sums.at[t], td(d)) for d in range(1, 8)]
+    on(r)
     for k in range(4):
         mom[0, k] = first[4 * k:4 * k + 4]
         mom[1, k] = second[4 * k:4 * k + 4]
-    nf_o[...] = mom[0, q]
-    ns_o[...] = mom[1, q]
-    for x in da:
-        x.wait_recv()
-    dy = [send(dall.at[p, y], dall.at[p, y], yd(d)) for d in YS for p in range(2)]
+    out_o[48:52, :] = mom[0, q]
+    out_o[52:56, :] = mom[1, q]
+    for x in st:
+        x.wait_recv()
+    s = sums[0]
+    for i in range(1, 8):
+        s = s + sums[i]
+    klass[r] = s
+    sa_copies = [send(klass.at[r], klass.at[r], zd(d)) for d in (1, 15, 2)]
+    for d in (1, 15):
+        for x in da[d]:
+            x.wait_recv()
+        on(lax.rem(z + 16 - d, 4))
+    for d in (2, 14):
+        for x in da[d]:
+            x.wait_recv()
+    on(lax.rem(z + 2, 4))
+    for x in sa_copies:
+        x.wait_recv()
+    ysum[y] = ((klass[0] + klass[1]) + klass[2]) + klass[3]
+    sy_copies = [send(ysum.at[y], ysum.at[y], yd(d)) for d in YS]
 
     grad = []
     for c in range(2):
@@ -192,43 +262,43 @@
             total = total + unpack(rb[c, j].astype(F32))
         grad.append(total)
     grad = jnp.concatenate(grad, axis=1)
+    mine = fac_p.astype(BF16)
+    in_w.wait()
 
     for x in dy:
         x.wait_recv()
-    both = []
-    for p in range(2):
-        both.append(dall[p].reshape(256, 512))
-        wide = both[p].astype(F32)
-        sq = (wide * wide).reshape(32, 8, 512).sum(axis=0)
-        sums[t, p] = sq[:, 0:128] + sq[:, 128:256] + sq[:, 256:384] + sq[:, 384:512]
-    st = [send(sums.at[t], sums.at[t], td(d)) for d in range(1, 8)]
-    mine = fac_p.astype(BF16)
+    both = [dall[p].reshape(256, 512) for p in range(2)]
     back_dir = jnp.dot(mine, both[0], preferred_element_type=F32)
     back_proj = jnp.dot(mine, both[1], preferred_element_type=F32)
-    for x in st:
-        x.wait_recv()
-    totals = []
-    for p in range(2):
-        s = sums[0, p]
-        for i in range(1, 8):
-            s = s + sums[i, p]
-        totals.append(jnp.sum(jnp.sum(s, axis=1, keepdims=True), axis=0, keepdims=True))
+    for x in sy_copies:
+        x.wait_recv()
+    s = ((ysum[0] + ysum[1]) + ysum[2]) + ysum[3]
+    totals = [jnp.sum(jnp.sum(s[p], axis=1, keepdims=True), axis=0, keepdims=True) for p in range(2)]
     scale = jnp.sqrt(totals[0]) / jnp.sqrt(totals[1] + 1e-06)
     update = back_dir + scale * (grad - back_proj)
-    up_o[...] = update
+    out_o[0:24, :] = update
     new_w = w[...] - 0.01 * update
-    nw_o[...] = new_w
+    out_o[24:48, :] = new_w
     wall[y, r, q] = jnp.concatenate([pack(new_w[:, 0:256]), pack(new_w[:, 256:512])], axis=1).astype(BF16)
 
     def block(dz, j):
         zz = lax.rem(z + 16 - dz, 16)
         return lax.rem(zz, 4), lax.rem(zz // 4 + 4 - j, 4)
 
-    last = []
-
-    def spread(rr, kk):
-        for d in YS:
-            last.append(send(wall.at[y, rr, kk], wall.at[y, rr, kk], yd(d)))
+    spread, onward = [], []
+
+    def to_y(rr, kk):
+        here = wall.at[y, rr, kk]
+        spread.append((send(here, here, yd(1)), send(here, here, yd(3)), rr, kk))
+
+    def pass_on(n):
+        for _ in range(n):
+            i = len(onward)
+            up, down, rr, kk = spread[i]
+            for c in (up, down):
+                c.wait_recv()
+            here = wall.at[lax.rem(y + (1 if i % 2 else 3), 4), rr, kk]
+            onward.append(send(here, here, yd(3 if i % 2 else 1)))
 
     first_b = {j: send(wall.at[y, r, q], wall.at[y, r, q], zd(4 * j)) for j in (2, 1, 3)}
     second_a = {}
@@ -238,26 +308,29 @@
         to = {0: (1, 15, 2, 14), 1: (1, 15, 2), 3: (1, 15, 14), 2: (1, 15)}[j]
         for d in to:
             second_a[j, d] = send(wall.at[y, rr, kk], wall.at[y, rr, kk], zd(d))
+        to_y(rr, kk)
         return to
 
     def landed(j, to):
         for d in to:
             second_a[j, d].wait_recv()
-            spread(*block(d, j))
-
-    to = around(0)
-    spread(r, q)
-    landed(0, to)
+            to_y(*block(d, j))
+
+    landed(0, around(0))
+    to = {}
     for j in (1, 3):
         first_b[j].wait_recv()
-        to = around(j)
-        spread(*block(0, j))
-        landed(j, to)
+        to[j] = around(j)
+    pass_on(1)
+    landed(1, to[1])
+    landed(3, to[3])
+    pass_on(4)
     first_b[2].wait_recv()
     to = around(2)
-    spread(*block(0, 2))
+    pass_on(2)
     landed(2, to)
-    for x in last:
+    pass_on(9)
+    for x in onward:
         x.wait_recv()
     for k in range(4):
         for rr in range(4):
@@ -267,24 +340,41 @@
                 v = wall[yy, rr, k].astype(F32)
                 out.append(jnp.concatenate([unpack(v[:, 0:384]), unpack(v[:, 384:768])], axis=1))
             wc_o[at:at + 96, :] = jnp.concatenate(out, axis=0).astype(BF16)
+    assert len(copies) <= N_SEM
     for x in copies:
         x.wait_send()
+
+
+def finish(small, wc, nw_o, up_o, nf_o, ns_o, wc_o):
+    up_o[...] = small[0:24, :]
+    nw_o[...] = small[24:48, :]
+    nf_o[...] = small[48:52, :]
+    ns_o[...] = small[52:56, :]
+    wc_o[...] = wc[...]
 
 
 def per_device(*args):
     v = pl.BlockSpec(memory_space=pltpu.VMEM)
     shape = jax.ShapeDtypeStruct
-    return pl.pallas_call(
+    small, wc = pl.pallas_call(
         kernel,
         name="step",
-        out_shape=(shape((24, 512), F32), shape((24, 512), F32), shape((4, 512), F32), shape((4, 512), F32),
-                   shape((1536, 512), BF16)),
-        in_specs=[v] * 6,
-        out_specs=[v] * 5,
+        out_shape=(shape((56, 512), F32), shape((1536, 512), BF16)),
+        in_specs=[pl.BlockSpec(memory_space=pl.ANY)] * 6,
+        out_specs=[v] * 2,
         scratch_shapes=[
+            pltpu.VMEM((1024, 1536), BF16),
+            pltpu.VMEM((1024, 512), BF16),
+            pltpu.VMEM((24, 256), BF16),
+            pltpu.VMEM((24, 512), F32),
+            pltpu.VMEM((2, 4, 4, 512), F32),
+            pltpu.VMEM((4, 384, 1024), BF16),
             pltpu.VMEM((2, 1536, 256), F32),
             pltpu.VMEM((2, 1536, 256), BF16),
-            pltpu.VMEM((2, 3, 384, 256), BF16),
+            pltpu.VMEM((2, 2, 192, 256), BF16),
+            pltpu.VMEM((2, 2, 192, 256), BF16),
+            pltpu.VMEM((2, 2, 192, 256), BF16),
+            pltpu.VMEM((2, 2, 192, 256), BF16),
             pltpu.VMEM((2, 384, 256), F32),
             pltpu.VMEM((2, 384, 256), BF16),
             pltpu.VMEM((2, 3, 96, 256), BF16),
@@ -303,14 +393,24 @@
             pltpu.VMEM((4, 4, 512), F32),
             pltpu.VMEM((2, 4, 4, 16, 512), BF16),
             pltpu.VMEM((2, 16, 512), F32),
-            pltpu.VMEM((2, 4, 4, 512), F32),
             pltpu.VMEM((8, 2, 8, 128), F32),
+            pltpu.VMEM((4, 2, 8, 128), F32),
+            pltpu.VMEM((4, 2, 8, 128), F32),
             pltpu.VMEM((4, 4, 4, 16, 768), BF16),
+            pltpu.SemaphoreType.DMA((9,)),
             pltpu.SemaphoreType.DMA((N_SEM,)),
             pltpu.SemaphoreType.DMA((N_SEM,)),
         ],
         compiler_params=pltpu.CompilerParams(collective_id=0, has_side_effects=True, vmem_limit_bytes=56 * 1024 * 1024),
     )(*args)
+    return pl.pallas_call(
+        finish,
+        name="finish",
+        out_shape=(shape((24, 512), F32), shape((24, 512), F32), shape((4, 512), F32), shape((4, 512), F32),
+                   shape((1536, 512), BF16)),
+        in_specs=[v] * 2,
+        out_specs=[v] * 5,
+    )(small, wc)
 
 
 def solution(mesh):

time: 113 us -> 97.9 us (0.87); the launches traced: 111 us -> 97.7 us
  local copies, waits for them, and re-layouts: 8.08 us -> 0 us
  Pallas kernels: 103 us -> 97.1 us
    unnamed x5 -> x0, local copies, waits for them, and re-layouts: 8.08 us -> none
    pallas_call x1 -> x2, Pallas kernels: 103 us -> 97.1 us  [the longest x1 94.3 us: per_device(): pl.pallas_call(kernel, name='step', out_shape=(shape((56, 512), F32), sha...]
where the time goes in v2:
time: 97.9 us; the launch traced here: 97.7 us
  Pallas kernels  97.1 us (99%)
    pallas_call x1, Pallas kernels, per_device(): pl.pallas_call(kernel, name='step', out_shape=(shape((56, 512), F32), sha...  94.3 us
    pallas_call x1, Pallas kernels, per_device(): pl.pallas_call(finish, name='finish', out_shape=(shape((24, 512), F32), s...  2.73 us

profile of v2, /device:TPU:24, one launch (start us, length us, event | category | flops | bytes accessed | tf_op | source)
XLA Modules:
  0.0 97.7 jit_solution(12560613009618239519)
XLA Ops:
  0.6 94.3 %step.1 = (f32[56,512]{1,0:T(8,128)}, bf16[1536,512]{1,0:T(8,128)(2,1)}) custom-call(bf16[1024,1536]{1,0:T(8,128)(2,1)} %mixer_h.1, bf16[1024,512]{1,0:T(8,128)(2,1)} %og_h.1, bf16[24,256]{1,0:T(8,128)(2,1)} %fac_h.1, f32[24,512]{1,0:T(8,128)} %w_h.1, f32[4,512]{1,0:T(4,128)} %m1_h.1, f32[4,512]{1,0:T(4,128)} %m2_h.1), custom_call_target="tpu_custom_call" | custom-call | tf_op jit(solution)/shard_map/step/pallas_call | solution.py:359
  95.0 2.7 %finish.1 = (f32[24,512]{1,0:T(8,128)}, f32[24,512]{1,0:T(8,128)}, f32[4,512]{1,0:T(4,128)}, f32[4,512]{1,0:T(4,128)}, bf16[1536,512]{1,0:T(8,128)(2,1)}) custom-call(f32[56,512]{1,0:T(8,128)} %get-tuple-element.7.small, bf16[1536,512]{1,0:T(8,128)(2,1)} %get-tuple-element.8.wc), custom_call_target="tpu_custom_call" | custom-call | tf_op jit(solution)/shard_map/finish/pallas_call | solution.py:406

commit v3 on v0

v3 whole, which is shorter than its diff:
```python
import jax
import jax.numpy as jnp
from jax import lax
from jax.experimental import pallas as pl
from jax.experimental.pallas import tpu as pltpu
from jax.sharding import PartitionSpec as P

MESH = pl.DeviceIdType.MESH
F32, BF16 = jnp.float32, jnp.bfloat16
WINDOW = ((1, 15, 2), (1, 15, 14))
YS = (1, 3, 2)
N_SEM = 224


def rows_dot(a, b):
    return lax.dot_general(a, b, (((0,), (0,)), ((), ())), preferred_element_type=F32)


def kernel(mixer_h, og_h, fac_h, w_h, m1_h, m2_h, out_o, wc_o,
           mixer, og, facy, fr, wv, wy, mv, my, mk, gf, sy, relay, direct, joined, landed_j, gy, sa, ra, ga, sb, rb,
           pp, rpa, pb, dall, pz, po, us, uo, sums, klass, wall, isem, ssem, rsem):
    z, y, t = lax.axis_index("fs"), lax.axis_index("rep"), lax.axis_index("tp")
    q, r = z // 4, lax.rem(z, 4)

    def zd(d):
        return {"fs": lax.rem(z + d, 16)}

    def yd(d):
        return {"rep": lax.rem(y + d, 4)}

    def td(d):
        return {"tp": lax.rem(t + d, 8)}

    def zyd(dz, dy):
        return {"fs": lax.rem(z + dz, 16), "rep": lax.rem(y + dy, 4)}

    copies = []

    def send(src, dst, dev):
        i = len(copies)
        c = pltpu.make_async_remote_copy(src_ref=src, dst_ref=dst, send_sem=ssem.at[i], recv_sem=rsem.at[i],
                                         device_id=dev, device_id_type=MESH)
        c.start()
        copies.append(c)
        return c

    def lanes(yy):
        return pl.ds(pl.multiple_of(yy * 128, 128), 128)

    barrier = pltpu.get_barrier_semaphore()
    peers = [zd(d) for d in (1, 15, 2, 14, 3, 13, 4, 12, 8)] + [yd(d) for d in YS] + [td(d) for d in range(1, 8)]
    peers += [zyd(dz, dy) for dz in (1, 15, 2, 14) for dy in YS]
    for dev in peers:
        pl.semaphore_signal(barrier, inc=1, device_id=dev, device_id_type=MESH)

    def load(i, src, dst):
        c = pltpu.make_async_copy(src, dst, isem.at[i])
        c.start()
        return c

    tiles = [pl.ds(384 * k, 384) for k in range(4)]
    in_og = load(0, og_h, og)
    in_mixer = [load(1 + k, mixer_h.at[:, tiles[k]], mixer.at[:, tiles[k]]) for k in range(4)]
    in_small = [load(5, fac_h, facy.at[y]), load(6, m1_h, mv.at[0]), load(7, m2_h, mv.at[1]), load(8, w_h, wv),
                load(9, m1_h.at[:, lanes(y)], my.at[0, y]), load(10, m2_h.at[:, lanes(y)], my.at[1, y]),
                load(11, w_h.at[:, lanes(y)], wy.at[y])]

    def partial(k):
        in_mixer[k].wait()
        tile = rows_dot(mixer[:, tiles[k]], og[...])
        for rr in range(4):
            for yy in range(4):
                v = tile[96 * rr:96 * rr + 96, 128 * yy:128 * yy + 128]
                gf[yy, k, rr] = v
                sy[yy, k, rr] = v.astype(BF16)

    in_og.wait()
    partial(0)
    partial(1)
    for x in in_small:
        x.wait()
    pl.semaphore_wait(barrier, len(peers))

    def at_y(d):
        return lax.rem(y + d, 4)

    def step_one(c):
        up = [send(sy.at[at_y(2), 2 * c], relay.at[c, 0], yd(1)), send(sy.at[at_y(1), 2 * c + 1], direct.at[c, 0], yd(1))]
        down = [send(sy.at[at_y(2), 2 * c + 1], relay.at[c, 1], yd(3)), send(sy.at[at_y(3), 2 * c], direct.at[c, 1], yd(3))]
        return up[0], down[0], up[1], down[1]

    def step_two(c, first):
        out = []
        for i, d in ((0, 1), (1, 3)):
            first[i].wait_recv()
            joined[c, i] = (gf[at_y(d), 2 * c + i] + relay[c, i].astype(F32)).astype(BF16)
            out.append(send(joined.at[c, i], landed_j.at[c, i], yd(d)))
        return list(first[2:]) + out

    fy = [send(facy.at[y], facy.at[y], yd(d)) for d in YS]
    ones, twos = [step_one(0), None], [None, None]
    my_copies = [send(mv.at[p, :, lanes(at_y(d))], my.at[p, y], yd(d)) for p in range(2) for d in YS]
    partial(2)
    partial(3)
    ones[1] = step_one(1)
    for x in fy:
        x.wait_recv()
    fz = jnp.concatenate([facy[yy].astype(F32) for yy in range(4)], axis=0).astype(BF16)
    fr[q] = fz
    fb = [send(fr.at[q], fr.at[q], zd(4 * j)) for j in (2, 1, 3)]
    twos[0] = step_two(0, ones[0])
    for x in my_copies:
        x.wait_recv()
    for p in range(2):
        for yy in range(4):
            mk[p, q, 4 * yy:4 * yy + 4, :] = my[p, yy]
    mb = [send(mk.at[p, q], mk.at[p, q], zd(4 * j)) for j in (2, 1, 3) for p in range(2)]
    twos[1] = step_two(1, ones[1])
    wy_copies = [send(wv.at[:, lanes(at_y(d))], wy.at[y], yd(d)) for d in YS]

    ga_copies = []
    for c in range(2):
        for x in twos[c]:
            x.wait_recv()
        for k, i, other in ((2 * c, 0, 1), (2 * c + 1, 1, 0)):
            total = gf[y, k] + landed_j[c, i].astype(F32) + direct[c, other].astype(F32)
            gy[k] = total
            sa[k] = total.astype(BF16)
        ga_copies.append([send(sa.at[pl.ds(2 * c, 2), lax.rem(z + d, 4)], ra.at[c, j], zd(d))
                          for j, d in enumerate(WINDOW[c])])

    for x in fb:
        x.wait_recv()
    part = None
    for c in range(2):
        for x in ga_copies[c]:
            x.wait_recv()
        for i in range(2):
            k = 2 * c + i
            total = gy[k, r]
            for j in range(3):
                total = total + ra[c, j, i].astype(F32)
            ga[k] = total
            low = total.astype(BF16)
            sb[k] = low
            add = rows_dot(fr[k], low) + rows_dot(fr[k], (total - low.astype(F32)).astype(BF16))
            part = add if part is None else part + add
    pp[...] = part.reshape(4, 4, 16, 128)
    pa_copies = [[send(pp.at[pl.ds(2 * h, 2), lax.rem(z + d, 4)], rpa.at[h, j], zd(d)) for j, d in enumerate(WINDOW[h])]
                 for h in range(2)]
    for h in range(2):
        for x in pa_copies[h]:
            x.wait_recv()
        for i in range(2):
            k = 2 * h + i
            pb[q, k] = (pp[k, r] + rpa[h, 0, i] + rpa[h, 1, i] + rpa[h, 2, i]).astype(BF16)
    pb_copies = [send(pb.at[q], pb.at[q], zd(4 * j)) for j in (2, 1, 3)]
    gb_copies = [send(sb.at[lax.rem(q + j, 4)], rb.at[j - 1], zd(4 * j)) for j in (2, 1, 3)]
    for x in mb:
        x.wait_recv()
    for x in pb_copies:
        x.wait_recv()
    proj = [jnp.concatenate([pb[i, k].astype(F32) for k in range(4)], axis=0) for i in range(4)]
    proj = ((proj[0] + proj[1]) + proj[2]) + proj[3]
    first = 0.8 * mk[0].reshape(64, 128) + 0.2 * proj
    second = 0.9 * mk[1].reshape(64, 128) + 0.1 * proj * proj
    low = [(first / (jnp.sqrt(second) + 1e-08)).astype(BF16), proj.astype(BF16)]
    for p in range(2):
        for k in range(4):
            dall[p, k, r] = low[p][16 * k:16 * k + 16]
        wide = low[p].astype(F32)
        sums[t, p] = jnp.sum((wide * wide).reshape(8, 8, 128), axis=0)
    st = [send(sums.at[t], sums.at[t], td(d)) for d in range(1, 8)]
    da = [send(dall.at[p, :, r], dall.at[p, :, r], zd(d)) for d in (1, 15) for p in range(2)]
    for d, at in ((2, 0), (14, 2)):
        for p in range(2):
            here = dall.at[p, pl.ds(at, 2), r]
            da.append(send(here, here, zd(d)))
    for k in range(4):
        for yy in range(4):
            pz[k, yy] = proj[16 * k + 4 * yy:16 * k + 4 * yy + 4]
    po[y] = pz[q, y]
    po_copies = [send(pz.at[q, at_y(d)], po.at[y], yd(d)) for d in YS]

    for x in st:
        x.wait_recv()
    s = sums[0]
    for i in range(1, 8):
        s = s + sums[i]
    klass[r, y] = s
    kl_copies = [send(klass.at[r, y], klass.at[r, y], zyd(dz, dy)) for dz in (2, 1, 15, 0) for dy in (2, 1, 3, 0)
                 if dz or dy]

    for x in wy_copies:
        x.wait_recv()
    weight = jnp.concatenate([wy[yy] for yy in range(4)], axis=0)
    for x in gb_copies:
        x.wait_recv()
    grad = ga[q]
    for j in range(3):
        grad = grad + rb[j].astype(F32)
    for x in da:
        x.wait_recv()
    back_dir = jnp.dot(fz, dall[0].reshape(256, 128), preferred_element_type=F32)
    back_proj = jnp.dot(fz, dall[1].reshape(256, 128), preferred_element_type=F32)
    for x in kl_copies:
        x.wait_recv()
    s = None
    for rr in range(4):
        for yy in range(4):
            s = klass[rr, yy] if s is None else s + klass[rr, yy]
    totals = [jnp.sum(jnp.sum(s[p], axis=1, keepdims=True), axis=0, keepdims=True) for p in range(2)]
    scale = jnp.sqrt(totals[0]) / jnp.sqrt(totals[1] + 1e-06)
    update = back_dir + scale * (grad - back_proj)
    wall[y, r, q] = (weight - 0.01 * update).astype(BF16)

    def of(delta):
        zz = lax.rem(z + 32 - delta, 16)
        return lax.rem(zz, 4), zz // 4

    spread, onward = [], []

    def to_y(rr, kk):
        here = wall.at[y, rr, kk]
        spread.append((send(here, here, yd(1)), send(here, here, yd(3)), rr, kk))

    def pass_on(n):
        for _ in range(n):
            i = len(onward)
            up, down, rr, kk = spread[i]
            for c in (up, down):
                c.wait_recv()
            here = wall.at[at_y(1 if i % 2 else 3), rr, kk]
            onward.append(send(here, here, yd(3 if i % 2 else 1)))

    near, far = {}, {}
    to_y(r, q)
    for m in (1, 4, 2, 3):
        for way in (1, -1):
            near[way, m] = send(wall.at[y, r, q], wall.at[y, r, q], zd(16 + way * m))
    for yy in range(4):
        us[yy] = update[24 * yy:24 * yy + 24]
    uo[y] = us[y]

    def landed(m):
        for way in (1, -1):
            near[way, m].wait_recv()
            rr, kk = of(4 * way)
            for n in (4, 1, 2, 3) if m == 4 else ():
                here = wall.at[y, rr, kk] if n < 4 else wall.at[y, rr, kk, pl.ds(24 - 24 * way, 48)]
                far[way, n] = send(here, here, zd(16 + way * n))
            to_y(*of(m * way))

    landed(1)
    landed(2)
    uo_copies = [send(us.at[at_y(d)], uo.at[y], yd(d)) for d in YS]
    landed(4)
    landed(3)
    pass_on(1)
    for n in (1, 2, 3):
        for way in (1, -1):
            far[way, n].wait_recv()
            to_y(*of((n + 4) * way))
        pass_on(2)
    for way in (1, -1):
        far[way, 4].wait_recv()
    to_y(*of(8))

    for x in uo_copies + po_copies:
        x.wait_recv()
    mine = jnp.concatenate([uo[yy] for yy in range(4)], axis=1)
    out_o[0:24, :] = mine
    out_o[24:48, :] = wv[...] - 0.01 * mine
    mine = jnp.concatenate([po[yy] for yy in range(4)], axis=1)
    out_o[48:52, :] = 0.8 * mv[0] + 0.2 * mine
    out_o[52:56, :] = 0.9 * mv[1] + 0.1 * mine * mine
    pass_on(9)
    for x in onward:
        x.wait_recv()
    for yy in range(4):
        for rr in range(4):
            for k in range(4):
                at = 96 * (4 * k + rr)
                wc_o[at:at + 96, 128 * yy:128 * yy + 128] = wall[yy, rr, k]
    assert len(copies) <= N_SEM
    for x in copies:
        x.wait_send()


def finish(small, wc, nw_o, up_o, nf_o, ns_o, wc_o):
    up_o[...] = small[0:24, :]
    nw_o[...] = small[24:48, :]
    nf_o[...] = small[48:52, :]
    ns_o[...] = small[52:56, :]
    wc_o[...] = wc[...]


def per_device(*args):
    v = pl.BlockSpec(memory_space=pltpu.VMEM)
    shape = jax.ShapeDtypeStruct
    small, wc = pl.pallas_call(
        kernel,
        name="step",
        out_shape=(shape((56, 512), F32), shape((1536, 512), BF16)),
        in_specs=[pl.BlockSpec(memory_space=pl.ANY)] * 6,
        out_specs=[v] * 2,
        scratch_shapes=[
            pltpu.VMEM((1024, 1536), BF16),
            pltpu.VMEM((1024, 512), BF16),
            pltpu.VMEM((4, 24, 256), BF16),
            pltpu.VMEM((4, 96, 256), BF16),
            pltpu.VMEM((24, 512), F32),
            pltpu.VMEM((4, 24, 128), F32),
            pltpu.VMEM((2, 4, 512), F32),
            pltpu.VMEM((2, 4, 4, 128), F32),
            pltpu.VMEM((2, 4, 16, 128), F32),
            pltpu.VMEM((4, 4, 4, 96, 128), F32),
            pltpu.VMEM((4, 4, 4, 96, 128), BF16),
            pltpu.VMEM((2, 2, 4, 96, 128), BF16),
            pltpu.VMEM((2, 2, 4, 96, 128), BF16),
            pltpu.VMEM((2, 2, 4, 96, 128), BF16),
            pltpu.VMEM((2, 2, 4, 96, 128), BF16),
            pltpu.VMEM((4, 4, 96, 128), F32),
            pltpu.VMEM((4, 4, 96, 128), BF16),
            pltpu.VMEM((2, 3, 2, 96, 128), BF16),
            pltpu.VMEM((4, 96, 128), F32),
            pltpu.VMEM((4, 96, 128), BF16),
            pltpu.VMEM((3, 96, 128), BF16),
            pltpu.VMEM((4, 4, 16, 128), F32),
            pltpu.VMEM((2, 3, 2, 16, 128), F32),
            pltpu.VMEM((4, 4, 16, 128), BF16),
            pltpu.VMEM((2, 4, 4, 16, 128), BF16),
            pltpu.VMEM((4, 4, 4, 128), F32),
            pltpu.VMEM((4, 4, 128), F32),
            pltpu.VMEM((4, 24, 128), F32),
            pltpu.VMEM((4, 24, 128), F32),
            pltpu.VMEM((8, 2, 8, 128), F32),
            pltpu.VMEM((4, 4, 2, 8, 128), F32),
            pltpu.VMEM((4, 4, 4, 96, 128), BF16),
            pltpu.SemaphoreType.DMA((12,)),
            pltpu.SemaphoreType.DMA((N_SEM,)),
            pltpu.SemaphoreType.DMA((N_SEM,)),
        ],
        compiler_params=pltpu.CompilerParams(collective_id=0, has_side_effects=True, vmem_limit_bytes=56 * 1024 * 1024),
    )(*args)
    return pl.pallas_call(
        finish,
        name="finish",
        out_shape=(shape((24, 512), F32), shape((24, 512), F32), shape((4, 512), F32), shape((4, 512), F32),
                   shape((1536, 512), BF16)),
        in_specs=[v] * 2,
        out_specs=[v] * 5,
    )(small, wc)


def solution(mesh):
    both = ("fs", "rep")
    in_specs = (P(both, None), P(both, "tp"), P(both, None), P(both, "tp"), P(both, "tp"), P(both, "tp"))
    out_specs = (P(both, "tp"), P(both, "tp"), P(both, "tp"), P(both, "tp"), P(None, "tp"))
    return jax.shard_map(per_device, mesh=mesh, in_specs=in_specs, out_specs=out_specs, check_vma=False)
```

time: 357 us -> 88.9 us (0.25)
  blocking collectives: 172 us -> 0 us
  waiting for transfers between devices: 145 us -> 0 us
  Pallas kernels: 0 us -> 88.2 us
  between operations: 15.5 us -> 0.64 us
  local copies, waits for them, and re-layouts: 9.04 us -> 0 us
  matrix products: 8.62 us -> 0 us
  other arithmetic: 4.95 us -> 0 us
    all_gather x2 -> x0, blocking collectives: 119 us -> none  [the longest x1 106 us: in_one_piece(): lax.all_gather(both, axis, axis=dim, tiled=True)]
    pallas_call x0 -> x2, Pallas kernels: none -> 88.2 us  [the longest x1 85.4 us: per_device(): pl.pallas_call(kernel, name='step', out_shape=(shape((56, 512), F32), sha...]
    reduce_scatter x1 -> x0, waiting for transfers between devices: 81.3 us -> none  [per_device(): lax.psum_scatter(contract_rows(columns, out_grad), 'fs', scatter_dimensio...]
    all_gather x1 -> x0, waiting for transfers between devices: 63.9 us -> none  [whole_of(): value = lax.all_gather(value, axis, axis=dim, tiled=True)]
    all_to_all x3 -> x0, blocking collectives: 53.6 us -> none  [the longest x2 44.3 us: sent_and_summed(): lax.all_to_all(in_blocks(value, dim, peers), axis, 0, 0, tiled=True)]
    dot_general x4 -> x0, matrix products: 8.62 us -> none  [the longest x2 5.78 us: contract_rows(): lax.dot_general(left, right, (((0,), (0,)), ((), ())), preferred_element_...]
    unnamed x12 -> x0, local copies, waits for them, and re-layouts: 6.47 us -> none
  transfers between devices with their start and end apart: 2 -> 0, of which waited for: 2 -> 0; matrix products, arithmetic and copies ran while one was open for 0% -> 0% of each run, Pallas kernels for 0% -> 0%
where the time goes in v3:
time: 88.9 us; the launch traced here: 88.8 us
  Pallas kernels  88.2 us (99%)
    pallas_call x1, Pallas kernels, per_device(): pl.pallas_call(kernel, name='step', out_shape=(shape((56, 512), F32), sha...  85.4 us
    pallas_call x1, Pallas kernels, per_device(): pl.pallas_call(finish, name='finish', out_shape=(shape((24, 512), F32), s...  2.73 us

profile of v3, /device:TPU:24, one launch (start us, length us, event | category | flops | bytes accessed | tf_op | source)
XLA Modules:
  0.0 88.8 jit_solution(13277279380663788078)
XLA Ops:
  0.6 85.4 %step.1 = (f32[56,512]{1,0:T(8,128)}, bf16[1536,512]{1,0:T(8,128)(2,1)}) custom-call(bf16[1024,1536]{1,0:T(8,128)(2,1)} %mixer_h.1, bf16[1024,512]{1,0:T(8,128)(2,1)} %og_h.1, bf16[24,256]{1,0:T(8,128)(2,1)} %fac_h.1, f32[24,512]{1,0:T(8,128)} %w_h.1, f32[4,512]{1,0:T(4,128)} %m1_h.1, f32[4,512]{1,0:T(4,128)} %m2_h.1), custom_call_target="tpu_custom_call" | custom-call | tf_op jit(solution)/shard_map/step/pallas_call | solution.py:301
  86.1 2.7 %finish.1 = (f32[24,512]{1,0:T(8,128)}, f32[24,512]{1,0:T(8,128)}, f32[4,512]{1,0:T(4,128)}, f32[4,512]{1,0:T(4,128)}, bf16[1536,512]{1,0:T(8,128)(2,1)}) custom-call(f32[56,512]{1,0:T(8,128)} %get-tuple-element.7.small, bf16[1536,512]{1,0:T(8,128)(2,1)} %get-tuple-element.8.wc), custom_call_target="tpu_custom_call" | custom-call | tf_op jit(solution)/shard_map/finish/pallas_call | solution.py:346

commit v4 on v3

--- a/solution.py
+++ b/solution.py
@@ -18,7 +18,7 @@
 
 def kernel(mixer_h, og_h, fac_h, w_h, m1_h, m2_h, out_o, wc_o,
            mixer, og, facy, fr, wv, wy, mv, my, mk, gf, sy, relay, direct, joined, landed_j, gy, sa, ra, ga, sb, rb,
-           pp, rpa, pb, dall, pz, po, us, uo, sums, klass, wall, isem, ssem, rsem):
+           pp, rpa, pb, dall, pz, po, us, uo, sums, klass, wall, isem, far_in, ssem, rsem):
     z, y, t = lax.axis_index("fs"), lax.axis_index("rep"), lax.axis_index("tp")
     q, r = z // 4, lax.rem(z, 4)
 
@@ -48,7 +48,7 @@
         return pl.ds(pl.multiple_of(yy * 128, 128), 128)
 
     barrier = pltpu.get_barrier_semaphore()
-    peers = [zd(d) for d in (1, 15, 2, 14, 3, 13, 4, 12, 8)] + [yd(d) for d in YS] + [td(d) for d in range(1, 8)]
+    peers = [zd(d) for d in (1, 15, 2, 14, 3, 13, 4, 12)] + [yd(d) for d in YS] + [td(d) for d in range(1, 8)]
     peers += [zyd(dz, dy) for dz in (1, 15, 2, 14) for dy in YS]
     for dev in peers:
         pl.semaphore_signal(barrier, inc=1, device_id=dev, device_id_type=MESH)
@@ -80,71 +80,79 @@
     for x in in_small:
         x.wait()
     pl.semaphore_wait(barrier, len(peers))
+    pl.semaphore_signal(far_in, inc=1, device_id=zd(4), device_id_type=MESH)
 
     def at_y(d):
         return lax.rem(y + d, 4)
 
-    def step_one(c):
-        up = [send(sy.at[at_y(2), 2 * c], relay.at[c, 0], yd(1)), send(sy.at[at_y(1), 2 * c + 1], direct.at[c, 0], yd(1))]
-        down = [send(sy.at[at_y(2), 2 * c + 1], relay.at[c, 1], yd(3)), send(sy.at[at_y(3), 2 * c], direct.at[c, 1], yd(3))]
+    halves = (pl.ds(0, 2), pl.ds(2, 2))
+
+    def step_one(k):
+        up = [send(sy.at[at_y(2), k, halves[0]], relay.at[k, 0], yd(1)), send(sy.at[at_y(1), k, halves[1]], direct.at[k, 0], yd(1))]
+        down = [send(sy.at[at_y(2), k, halves[1]], relay.at[k, 1], yd(3)), send(sy.at[at_y(3), k, halves[0]], direct.at[k, 1], yd(3))]
         return up[0], down[0], up[1], down[1]
 
-    def step_two(c, first):
+    def step_two(k, first):
         out = []
         for i, d in ((0, 1), (1, 3)):
             first[i].wait_recv()
-            joined[c, i] = (gf[at_y(d), 2 * c + i] + relay[c, i].astype(F32)).astype(BF16)
-            out.append(send(joined.at[c, i], landed_j.at[c, i], yd(d)))
+            joined[k, i] = (gf[at_y(d), k, halves[i]] + relay[k, i].astype(F32)).astype(BF16)
+            out.append(send(joined.at[k, i], landed_j.at[k, i], yd(d)))
         return list(first[2:]) + out
 
     fy = [send(facy.at[y], facy.at[y], yd(d)) for d in YS]
-    ones, twos = [step_one(0), None], [None, None]
+    ones, twos, ga_copies = [step_one(0), step_one(1)], [], []
     my_copies = [send(mv.at[p, :, lanes(at_y(d))], my.at[p, y], yd(d)) for p in range(2) for d in YS]
     partial(2)
     partial(3)
-    ones[1] = step_one(1)
     for x in fy:
         x.wait_recv()
     fz = jnp.concatenate([facy[yy].astype(F32) for yy in range(4)], axis=0).astype(BF16)
     fr[q] = fz
+    pl.semaphore_wait(far_in, 1)
     fb = [send(fr.at[q], fr.at[q], zd(4 * j)) for j in (2, 1, 3)]
-    twos[0] = step_two(0, ones[0])
+    twos.append(step_two(0, ones[0]))
+    ones.append(step_one(2))
     for x in my_copies:
         x.wait_recv()
     for p in range(2):
         for yy in range(4):
             mk[p, q, 4 * yy:4 * yy + 4, :] = my[p, yy]
     mb = [send(mk.at[p, q], mk.at[p, q], zd(4 * j)) for j in (2, 1, 3) for p in range(2)]
-    twos[1] = step_two(1, ones[1])
-    wy_copies = [send(wv.at[:, lanes(at_y(d))], wy.at[y], yd(d)) for d in YS]
-
-    ga_copies = []
-    for c in range(2):
-        for x in twos[c]:
-            x.wait_recv()
-        for k, i, other in ((2 * c, 0, 1), (2 * c + 1, 1, 0)):
-            total = gf[y, k] + landed_j[c, i].astype(F32) + direct[c, other].astype(F32)
-            gy[k] = total
-            sa[k] = total.astype(BF16)
-        ga_copies.append([send(sa.at[pl.ds(2 * c, 2), lax.rem(z + d, 4)], ra.at[c, j], zd(d))
-                          for j, d in enumerate(WINDOW[c])])
-
-    for x in fb:
-        x.wait_recv()
-    part = None
-    for c in range(2):
-        for x in ga_copies[c]:
+    twos.append(step_two(1, ones[1]))
+    ones.append(step_one(3))
+
+    def stage_a(k):
+        for x in twos[k]:
             x.wait_recv()
         for i in range(2):
-            k = 2 * c + i
-            total = gy[k, r]
-            for j in range(3):
-                total = total + ra[c, j, i].astype(F32)
-            ga[k] = total
-            low = total.astype(BF16)
-            sb[k] = low
-            add = rows_dot(fr[k], low) + rows_dot(fr[k], (total - low.astype(F32)).astype(BF16))
-            part = add if part is None else part + add
+            total = gf[y, k, halves[i]] + landed_j[k, i].astype(F32) + direct[k, 1 - i].astype(F32)
+            gy[k, halves[i]] = total
+            sa[k, halves[i]] = total.astype(BF16)
+        ga_copies.append([send(sa.at[k, lax.rem(z + d, 4)], ra.at[k, j], zd(d)) for j, d in enumerate(WINDOW[k % 2])])
+
+    stage_a(0)
+    twos.append(step_two(2, ones[2]))
+    stage_a(1)
+    twos.append(step_two(3, ones[3]))
+    wy_copies = [send(wv.at[:, lanes(at_y(d))], wy.at[y], yd(d)) for d in YS]
+    stage_a(2)
+    stage_a(3)
+
+    for x in fb:
+        x.wait_recv()
+    part = None
+    for k in range(4):
+        for x in ga_copies[k]:
+            x.wait_recv()
+        total = gy[k, r]
+        for j in range(3):
+            total = total + ra[k, j].astype(F32)
+        ga[k] = total
+        low = total.astype(BF16)
+        sb[k] = low
+        add = rows_dot(fr[k], low) + rows_dot(fr[k], (total - low.astype(F32)).astype(BF16))
+        part = add if part is None else part + add
     pp[...] = part.reshape(4, 4, 16, 128)
     pa_copies = [[send(pp.at[pl.ds(2 * h, 2), lax.rem(z + d, 4)], rpa.at[h, j], zd(d)) for j, d in enumerate(WINDOW[h])]
                  for h in range(2)]
@@ -165,11 +173,14 @@
     first = 0.8 * mk[0].reshape(64, 128) + 0.2 * proj
     second = 0.9 * mk[1].reshape(64, 128) + 0.1 * proj * proj
     low = [(first / (jnp.sqrt(second) + 1e-08)).astype(BF16), proj.astype(BF16)]
+    squares = []
     for p in range(2):
         for k in range(4):
             dall[p, k, r] = low[p][16 * k:16 * k + 16]
         wide = low[p].astype(F32)
-        sums[t, p] = jnp.sum((wide * wide).reshape(8, 8, 128), axis=0)
+        sq = jnp.sum((wide * wide).reshape(8, 8, 128), axis=0)
+        squares.append(sq[0:4] + sq[4:8])
+    sums[t] = jnp.concatenate(squares, axis=0)
     st = [send(sums.at[t], sums.at[t], td(d)) for d in range(1, 8)]
     da = [send(dall.at[p, :, r], dall.at[p, :, r], zd(d)) for d in (1, 15) for p in range(2)]
     for d, at in ((2, 0), (14, 2)):
@@ -209,7 +220,7 @@
     for rr in range(4):
         for yy in range(4):
             s = klass[rr, yy] if s is None else s + klass[rr, yy]
-    totals = [jnp.sum(jnp.sum(s[p], axis=1, keepdims=True), axis=0, keepdims=True) for p in range(2)]
+    totals = [jnp.sum(jnp.sum(s[4 * p:4 * p + 4], axis=1, keepdims=True), axis=0, keepdims=True) for p in range(2)]
     scale = jnp.sqrt(totals[0]) / jnp.sqrt(totals[1] + 1e-06)
     update = back_dir + scale * (grad - back_proj)
     wall[y, r, q] = (weight - 0.01 * update).astype(BF16)
@@ -287,12 +298,14 @@
         x.wait_send()
 
 
-def finish(small, wc, nw_o, up_o, nf_o, ns_o, wc_o):
-    up_o[...] = small[0:24, :]
-    nw_o[...] = small[24:48, :]
-    nf_o[...] = small[48:52, :]
-    ns_o[...] = small[52:56, :]
-    wc_o[...] = wc[...]
+def finish(small, wc, nw_o, up_o, nf_o, ns_o, wc_o, sem):
+    moves = ((wc, wc_o), (small.at[0:24, :], up_o), (small.at[24:48, :], nw_o), (small.at[48:52, :], nf_o),
+             (small.at[52:56, :], ns_o))
+    copies = [pltpu.make_async_copy(src, dst, sem.at[i]) for i, (src, dst) in enumerate(moves)]
+    for c in copies:
+        c.start()
+    for c in copies:
+        c.wait()
 
 
 def per_device(*args):
@@ -301,7 +314,7 @@
     small, wc = pl.pallas_call(
         kernel,
         name="step",
-        out_shape=(shape((56, 512), F32), shape((1536, 512), BF16)),
+        out_shape=(pltpu.VMEM((56, 512), F32), pltpu.VMEM((1536, 512), BF16)),
         in_specs=[pl.BlockSpec(memory_space=pl.ANY)] * 6,
         out_specs=[v] * 2,
         scratch_shapes=[
@@ -316,13 +329,13 @@
             pltpu.VMEM((2, 4, 16, 128), F32),
             pltpu.VMEM((4, 4, 4, 96, 128), F32),
             pltpu.VMEM((4, 4, 4, 96, 128), BF16),
-            pltpu.VMEM((2, 2, 4, 96, 128), BF16),
-            pltpu.VMEM((2, 2, 4, 96, 128), BF16),
-            pltpu.VMEM((2, 2, 4, 96, 128), BF16),
-            pltpu.VMEM((2, 2, 4, 96, 128), BF16),
+            pltpu.VMEM((4, 2, 2, 96, 128), BF16),
+            pltpu.VMEM((4, 2, 2, 96, 128), BF16),
+            pltpu.VMEM((4, 2, 2, 96, 128), BF16),
+            pltpu.VMEM((4, 2, 2, 96, 128), BF16),
             pltpu.VMEM((4, 4, 96, 128), F32),
             pltpu.VMEM((4, 4, 96, 128), BF16),
-            pltpu.VMEM((2, 3, 2, 96, 128), BF16),
+            pltpu.VMEM((4, 3, 96, 128), BF16),
             pltpu.VMEM((4, 96, 128), F32),
             pltpu.VMEM((4, 96, 128), BF16),
             pltpu.VMEM((3, 96, 128), BF16),
@@ -334,10 +347,11 @@
             pltpu.VMEM((4, 4, 128), F32),
             pltpu.VMEM((4, 24, 128), F32),
             pltpu.VMEM((4, 24, 128), F32),
-            pltpu.VMEM((8, 2, 8, 128), F32),
-            pltpu.VMEM((4, 4, 2, 8, 128), F32),
+            pltpu.VMEM((8, 8, 128), F32),
+            pltpu.VMEM((4, 4, 8, 128), F32),
             pltpu.VMEM((4, 4, 4, 96, 128), BF16),
             pltpu.SemaphoreType.DMA((12,)),
+            pltpu.SemaphoreType.REGULAR,
             pltpu.SemaphoreType.DMA((N_SEM,)),
             pltpu.SemaphoreType.DMA((N_SEM,)),
         ],
@@ -348,9 +362,10 @@
         name="finish",
         out_shape=(shape((24, 512), F32), shape((24, 512), F32), shape((4, 512), F32), shape((4, 512), F32),
                    shape((1536, 512), BF16)),
-        in_specs=[v] * 2,
-        out_specs=[v] * 5,
-    )(small, wc)
+        in_specs=[pl.BlockSpec(memory_space=pl.ANY)] * 2,
+        out_specs=[pl.BlockSpec(memory_space=pl.ANY)] * 5,
+        scratch_shapes=[pltpu.SemaphoreType.DMA((5,))],
+    )(pltpu.with_memory_space_constraint(small, pltpu.VMEM), pltpu.with_memory_space_constraint(wc, pltpu.VMEM))
 
 
 def solution(mesh):

time: 88.9 us -> 83.9 us (0.944)
  Pallas kernels: 88.2 us -> 83.1 us
    pallas_call x1, Pallas kernels: 85.4 us -> 81.9 us  [per_device(): pl.pallas_call(kernel, name='step', out_shape=(pltpu.VMEM((56, 512), F32)...]
    pallas_call x1, Pallas kernels: 2.73 us -> 1.2 us  [per_device(): pl.pallas_call(finish, name='finish', out_shape=(shape((24, 512), F32), s...]
where the time goes in v4:
time: 83.9 us; the launch traced here: 83.7 us
  Pallas kernels  83.1 us (99%)
    pallas_call x1, Pallas kernels, per_device(): pl.pallas_call(kernel, name='step', out_shape=(pltpu.VMEM((56, 512), F32)...  81.9 us

profile of v4, /device:TPU:24, one launch (start us, length us, event | category | flops | bytes accessed | tf_op | source)
XLA Modules:
  0.0 83.7 jit_solution(12006532634173935393)
XLA Ops:
  0.6 81.9 %step.1 = (f32[56,512]{1,0:T(8,128)S(1)}, bf16[1536,512]{1,0:T(8,128)(2,1)S(1)}) custom-call(bf16[1024,1536]{1,0:T(8,128)(2,1)} %mixer_h.1, bf16[1024,512]{1,0:T(8,128)(2,1)} %og_h.1, bf16[24,256]{1,0:T(8,128)(2,1)} %fac_h.1, f32[24,512]{1,0:T(8,128)} %w_h.1, f32[4,512]{1,0:T(4,128)} %m1_h.1, f32[4,512]{1,0:T(4,128)} %m2_h.1), custom_call_target="tpu_custom_call" | custom-call | tf_op jit(solution)/shard_map/step/pallas_call | solution.py:314
  82.5 1.2 %finish.1 = (f32[24,512]{1,0:T(8,128)}, f32[24,512]{1,0:T(8,128)}, f32[4,512]{1,0:T(4,128)}, f32[4,512]{1,0:T(4,128)}, bf16[1536,512]{1,0:T(8,128)(2,1)}) custom-call(f32[56,512]{1,0:T(8,128)S(1)} %get-tuple-element.7.small, bf16[1536,512]{1,0:T(8,128)(2,1)S(1)} %get-tuple-element.8.wc), custom_call_target="tpu_custom_call" | custom-call | tf_op jit(solution)/shard_map/finish/pallas_call | solution.py:360

commit v5 on v4

--- a/solution.py
+++ b/solution.py
@@ -285,14 +285,19 @@
     mine = jnp.concatenate([po[yy] for yy in range(4)], axis=1)
     out_o[48:52, :] = 0.8 * mv[0] + 0.2 * mine
     out_o[52:56, :] = 0.9 * mv[1] + 0.1 * mine * mine
-    pass_on(9)
-    for x in onward:
-        x.wait_recv()
-    for yy in range(4):
+    def write(d):
         for rr in range(4):
             for k in range(4):
                 at = 96 * (4 * k + rr)
-                wc_o[at:at + 96, 128 * yy:128 * yy + 128] = wall[yy, rr, k]
+                wc_o[at:at + 96, lanes(at_y(d))] = wall[at_y(d), rr, k]
+
+    write(0)
+    pass_on(9)
+    write(1)
+    write(3)
+    for x in onward:
+        x.wait_recv()
+    write(2)
     assert len(copies) <= N_SEM
     for x in copies:
         x.wait_send()

time: 83.9 us -> 83.7 us (level)
  no operation moved by 1% of the time
where the time goes in v5:
time: 83.7 us; the launch traced here: 83.5 us
  Pallas kernels  82.9 us (99%)
    pallas_call x1, Pallas kernels, per_device(): pl.pallas_call(kernel, name='step', out_shape=(pltpu.VMEM((56, 512), F32)...  81.7 us

profile of v5, /device:TPU:24, one launch (start us, length us, event | category | flops | bytes accessed | tf_op | source)
XLA Modules:
  0.0 83.5 jit_solution(14384006926929725388)
XLA Ops:
  0.6 81.7 %step.1 = (f32[56,512]{1,0:T(8,128)S(1)}, bf16[1536,512]{1,0:T(8,128)(2,1)S(1)}) custom-call(bf16[1024,1536]{1,0:T(8,128)(2,1)} %mixer_h.1, bf16[1024,512]{1,0:T(8,128)(2,1)} %og_h.1, bf16[24,256]{1,0:T(8,128)(2,1)} %fac_h.1, f32[24,512]{1,0:T(8,128)} %w_h.1, f32[4,512]{1,0:T(4,128)} %m1_h.1, f32[4,512]{1,0:T(4,128)} %m2_h.1), custom_call_target="tpu_custom_call" | custom-call | tf_op jit(solution)/shard_map/step/pallas_call | solution.py:319
  82.3 1.2 %finish.1 = (f32[24,512]{1,0:T(8,128)}, f32[24,512]{1,0:T(8,128)}, f32[4,512]{1,0:T(4,128)}, f32[4,512]{1,0:T(4,128)}, bf16[1536,512]{1,0:T(8,128)(2,1)}) custom-call(f32[56,512]{1,0:T(8,128)S(1)} %get-tuple-element.7.small, bf16[1536,512]{1,0:T(8,128)(2,1)S(1)} %get-tuple-element.8.wc), custom_call_target="tpu_custom_call" | custom-call | tf_op jit(solution)/shard_map/finish/pallas_call | solution.py:365
